TPU v7x, 32 devices: a whole 2x2x4 slice. The times are simulated.
32 devices in a mesh: ep: 4 (over y, x), tp: 8 (over z, core).
Axes of the slice: x: 2, y: 2, z: 4, core: 2. Of those that a mesh axis runs over, the one named last changes fastest.
Arguments:
- tokens: bfloat16 [64, 2048], P('ep', 'tp'), may hold values from -6 to 6
- key_cache: bfloat16 [64, 16, 1024, 128], P('ep', 'tp'), may hold values from -1700 to 1700
- value_cache: bfloat16 [64, 16, 1024, 128], P('ep', 'tp'), may hold values from -6 to 6
- gate_totals: float32 [64, 16, 1024], P('ep', 'tp'), as said below
- lengths: int32 [64], P('ep'), may hold values from 128 to 1024
- attn_gain: float32 [2048], replicated, may hold values from 0.1 to 1.9
- w_query: bfloat16 [2048, 2048], P(None, 'tp'), may hold values from -0.125 to 0.125
- w_key: bfloat16 [2048, 2048], P(None, 'tp'), may hold values from -0.125 to 0.125
- w_value: bfloat16 [2048, 2048], P(None, 'tp'), may hold values from -0.125 to 0.125
- w_forget: bfloat16 [2048, 16], replicated, may hold values from -0.125 to 0.125
- forget_bias: float32 [16], replicated, may hold values from -3 to 0
- w_attn_out: bfloat16 [2048, 2048], P('tp'), may hold values from -0.1875 to 0.1875
- moe_gain: float32 [2048], replicated, may hold values from 0.1 to 1.9
- group_ids: int32 [64, 1], P('ep'), may hold values from 0 to 3; in each aligned block of 16 rows (0 to 15, 16 to 31, ...) at most 8 rows name the same one
- inner_ids: int32 [64, 2], P('ep'), may hold values from 0 to 3, all different within a row
- group_prob: float32 [64], P('ep'), may hold values from 0.2 to 1
- pair_logits: float32 [64, 2], P('ep'), may hold values from -6 to 6
- w_expert_gate: bfloat16 [4, 2048, 2048], P('ep', None, 'tp'), may hold values from -0.125 to 0.125
- w_expert_up: bfloat16 [4, 2048, 2048], P('ep', None, 'tp'), may hold values from -0.125 to 0.125
- w_expert_down: bfloat16 [4, 2048, 2048], P('ep', 'tp'), may hold values from -0.375 to 0.375
- w_dense_in: bfloat16 [2048, 2048], P(None, 'tp'), may hold values from -0.125 to 0.125
- w_dense_out: bfloat16 [2048, 2048], P('tp'), may hold values from -0.1875 to 0.1875
- dense_gate: float32 [2048], P('tp'), may hold values from -2 to 2
Outputs:
- layer_output: bfloat16 [64, 2048], P('ep', 'tp')
- new_keys: bfloat16 [64, 16, 128], P('ep', 'tp')
- new_values: bfloat16 [64, 16, 128], P('ep', 'tp')
- new_gates: float32 [64, 16], P('ep', 'tp')
Inputs may be any that keep to these rules, and one draw needn't show every extreme that they name: `group_ids`: within the 16 sequences of each index of ep (aligned blocks of rows), no group is named by more than 8 sequences, a bound that some block reaches. `inner_ids`: each row names 2 different experts of its group. `gate_totals`: along positions the values of each sequence and head never rise.
All inputs are finite; a program needn't handle non-finite values.
Results may differ from a plain program's by a relative error of at most 0.011.
Values may be sent and summed in bfloat16 or wider, within the bound.
A program may use at most 64 MiB of HBM per device.

v0:
```python
import jax
import jax.numpy as jnp
from jax import lax
from jax.sharding import PartitionSpec as P

FFE = 512
EPG = 4


EPS = 1e-06
FLOOR = -1e30


def norm_rows(row_data, gain_vec):
    values = row_data.astype(jnp.float32)
    factor = lax.rsqrt(jnp.mean(values * values, axis=-1, keepdims=True) + EPS)
    return (values * factor * gain_vec).astype(jnp.bfloat16)


def head_norm(values):
    factor = lax.rsqrt(jnp.mean(values * values, axis=-1, keepdims=True) + EPS)
    return (values * factor).astype(jnp.bfloat16)


def attend(queries, fresh_key, fresh_value, key_cache, value_cache, gate_totals, lengths, current):
    score_scale = queries.shape[-1] ** (-0.5)
    scores = (
        jnp.einsum("shd,shld->shl", queries, key_cache, preferred_element_type=jnp.float32)
        * score_scale
    )
    scores = scores + current[:, :, None] - gate_totals
    entry_indices = jnp.arange(key_cache.shape[2])
    live_mask = (entry_indices[None, :] < lengths[:, None])[:, None, :]
    scores = jnp.where(live_mask, scores, FLOOR)
    own_score = (
        jnp.sum(queries.astype(jnp.float32) * fresh_key.astype(jnp.float32), axis=-1) * score_scale
    )
    peak = jnp.maximum(jnp.max(scores, axis=-1), own_score)
    expo_terms = jnp.where(live_mask, jnp.exp(scores - peak[:, :, None]), 0.0)
    own_expo = jnp.exp(own_score - peak)
    denom_sum = jnp.sum(expo_terms, axis=-1) + own_expo
    weights = (expo_terms / denom_sum[:, :, None]).astype(jnp.bfloat16)
    own_weight = (own_expo / denom_sum).astype(jnp.bfloat16)
    attended = jnp.einsum("shl,shld->shd", weights, value_cache, preferred_element_type=jnp.float32)
    attended = attended + own_weight.astype(jnp.float32)[:, :, None] * fresh_value.astype(
        jnp.float32
    )
    return attended.astype(jnp.bfloat16)


def body(
    tokens,
    key_cache,
    value_cache,
    gate_totals,
    lengths,
    attn_gain,
    w_query,
    w_key,
    w_value,
    w_forget,
    forget_bias,
    w_attn_out,
    moe_gain,
    group_ids,
    inner_ids,
    group_prob,
    pair_logits,
    w_expert_gate,
    w_expert_up,
    w_expert_down,
    w_dense_in,
    w_dense_out,
    dense_gate,
):
    gathered = lax.all_gather(tokens, "tp", axis=1, tiled=True)
    normed = norm_rows(gathered, attn_gain)
    seq_count = gathered.shape[0]
    heads_dev = key_cache.shape[1]
    head_dim = key_cache.shape[3]

    def project(weight):
        return jnp.dot(normed, weight, preferred_element_type=jnp.float32).reshape(
            seq_count, heads_dev, head_dim
        )

    queries = head_norm(project(w_query))
    new_keys = head_norm(project(w_key))
    new_values = project(w_value).astype(jnp.bfloat16)
    first_head = lax.axis_index("tp") * heads_dev
    forget_cols = lax.dynamic_slice_in_dim(w_forget, first_head, heads_dev, 1)
    forget_shift = lax.dynamic_slice_in_dim(forget_bias, first_head, heads_dev, 0)
    log_gate = jax.nn.log_sigmoid(
        jnp.dot(normed, forget_cols, preferred_element_type=jnp.float32) + forget_shift
    )
    entry_indices = jnp.arange(gate_totals.shape[2])
    at_last = (entry_indices[None, :] == (lengths - 1)[:, None])[:, None, :]
    new_gates = jnp.sum(jnp.where(at_last, gate_totals, 0.0), axis=2) + log_gate
    attended = attend(
        queries, new_keys, new_values, key_cache, value_cache, gate_totals, lengths, new_gates
    )
    partial_value = jnp.dot(
        attended.reshape(seq_count, heads_dev * head_dim),
        w_attn_out,
        preferred_element_type=jnp.float32,
    )
    piece_sum = lax.psum_scatter(partial_value, "tp", scatter_dimension=1, tiled=True)
    own_residual = (tokens.astype(jnp.float32) + piece_sum).astype(jnp.bfloat16)
    moe_in = norm_rows(lax.all_gather(own_residual, "tp", axis=1, tiled=True), moe_gain)
    groups = lax.axis_size("ep")
    capacity = max(2, 2 * seq_count // groups)
    first_share = jax.nn.sigmoid(pair_logits[:, 0] - pair_logits[:, 1])
    pair_share = group_prob[:, None] * jnp.stack([first_share, 1.0 - first_share], axis=1)
    inner_range = jnp.arange(EPG)
    spread = jnp.sum(
        jnp.where(inner_ids[:, :, None] == inner_range[None, None, :], pair_share[:, :, None], 0.0),
        axis=1,
    ).astype(jnp.bfloat16)
    choose = (group_ids == jnp.arange(groups)[None, :]).astype(jnp.int32)
    before = jnp.cumsum(choose, axis=0) - choose
    slot_of = group_ids[:, 0] * capacity + jnp.sum(before * choose, axis=1)
    slot_ids = jnp.arange(groups * capacity)
    send_map = (slot_of[None, :] == slot_ids[:, None]).astype(jnp.bfloat16)
    send_weights = jnp.dot(send_map, spread, preferred_element_type=jnp.float32).astype(
        jnp.bfloat16
    )
    send_rows = jnp.dot(send_map, moe_in, preferred_element_type=jnp.float32).astype(jnp.bfloat16)
    recv_rows, recv_weights = (
        lax.all_to_all(send_rows, "ep", split_axis=0, concat_axis=0, tiled=True),
        lax.all_to_all(send_weights, "ep", split_axis=0, concat_axis=0, tiled=True),
    )
    dense_hidden = jax.nn.silu(
        jnp.dot(moe_in, w_dense_in, preferred_element_type=jnp.float32)
    ).astype(jnp.bfloat16)
    dense_part = jnp.dot(dense_hidden, w_dense_out, preferred_element_type=jnp.float32)
    hidden_dev = w_expert_gate.shape[2]
    expert_index = lax.axis_index("tp") * hidden_dev // FFE
    route_col = jnp.sum(
        jnp.where(inner_range[None, :] == expert_index, recv_weights.astype(jnp.float32), 0.0),
        axis=1,
    )
    gate_pre = jnp.dot(recv_rows, w_expert_gate[0], preferred_element_type=jnp.float32)
    up_pre = jnp.dot(recv_rows, w_expert_up[0], preferred_element_type=jnp.float32)
    hidden = (jax.nn.silu(gate_pre) * up_pre * route_col[:, None]).astype(jnp.bfloat16)
    expert_part = jnp.dot(hidden, w_expert_down[0], preferred_element_type=jnp.float32)
    expert_sum, dense_sum = (
        lax.psum_scatter(expert_part, "tp", scatter_dimension=1, tiled=True),
        lax.psum_scatter(dense_part, "tp", scatter_dimension=1, tiled=True),
    )
    returned = lax.all_to_all(
        expert_sum.astype(jnp.bfloat16), "ep", split_axis=0, concat_axis=0, tiled=True
    )
    expert_out = lax.dot_general(
        send_map, returned, (((0,), (0,)), ((), ())), preferred_element_type=jnp.float32
    )
    layer_output = (
        own_residual.astype(jnp.float32) + expert_out + jax.nn.sigmoid(dense_gate) * dense_sum
    )
    return (layer_output.astype(jnp.bfloat16), new_keys, new_values, new_gates)


def solution(mesh):
    placed = (
        P("ep", "tp"),
        P("ep", "tp", None, None),
        P("ep", "tp", None, None),
        P("ep", "tp", None),
        P("ep"),
        P(),
        P(None, "tp"),
        P(None, "tp"),
        P(None, "tp"),
        P(),
        P(),
        P("tp", None),
        P(),
        P("ep", None),
        P("ep", None),
        P("ep"),
        P("ep", None),
        P("ep", None, "tp"),
        P("ep", None, "tp"),
        P("ep", "tp", None),
        P(None, "tp"),
        P("tp", None),
        P("tp"),
    )
    return jax.shard_map(
        body,
        mesh=mesh,
        in_specs=placed,
        out_specs=(P("ep", "tp"), P("ep", "tp", None), P("ep", "tp", None), P("ep", "tp")),
        check_vma=False,
    )
```

profile of v0, /device:TPU:0, one launch (start us, length us, event | category | flops | bytes accessed | tf_op | source)
XLA Modules:
  0.0 172.8 jit_solution(14352880859179264883)
XLA Ops:
  7.2 0.0 copy-start
  7.2 0.0 copy-start.5
  7.2 0.0 copy-start.4
  7.2 0.0 reduce-scatter.4.cloned.1.call-start
  7.3 0.8 broadcast_add_fusion
  8.1 0.7 iota_compare_fusion.1
  8.8 15.9 %all_gather.6 = bf16[16,2048]{1,0:T(8,128)(2,1)S(1)} all-gather(bf16[16,256]{1,0:T(8,128)(2,1)} %param.23), channel_id=1, replica_groups=mesh['ep'=4,'tp'=8] {'tp'}, dimensions={1}, use_global_device_ids=true | all-gather | bytes 73728 | tf_op jit(solution)/shard_map/all_gather | solution.py:76
  24.7 0.1 fusion.12
  24.8 1.5 fusion.67
  26.4 0.1 multiply_reduce_fusion.1
  26.5 1.5 fusion.70
  28.0 0.1 multiply_reduce_fusion.2
  28.1 0.1 iota_compare_fusion
  28.2 1.1 select_reduce_fusion
  29.3 0.1 copy.45
  29.4 0.7 dynamic_slice.7
  30.1 1.0 fusion.58
  31.1 0.0 copy-start.11
  31.1 0.1 copy.46
  31.2 0.7 multiply_reduce_fusion
  31.9 5.6 %fusion.34 = f32[16,2,1,1024]{3,2,1,0:T(1,128)S(1)} fusion(bf16[16,2,1024,128]{3,2,1,0:T(8,128)(2,1)} %param.24, bf16[16,2,128,1]{2,1,0,3:T(2,128)(2,1)S(1)} %get-tuple-element.12), kind=kOutput, calls=%fused_computation.48 | convolution fusion | flops 8388608 | bytes 8527872 | tf_op jit(solution)/shard_map/shd,shld->shl/dot_general | solution.py:28
  37.6 0.0 copy-start.14
  37.6 0.0 copy-start.10
  37.6 0.0 copy-start.8
  37.6 0.0 copy-start.6
  37.6 0.3 fusion.72
  37.9 0.3 fusion.32
  38.2 0.3 fusion.26
  38.5 0.3 convolution_convert_fusion.1
  38.8 0.0 copy-start.7
  38.8 0.0 copy-start.1
  38.8 0.0 copy-start.2
  38.9 0.0 copy-start.13
  38.9 4.7 %fusion.24 = f32[16,2,1,128]{3,2,1,0:T(1,128)S(1)} fusion(bf16[16,2,1024,128]{3,2,1,0:T(8,128)(2,1)} %param.25, bf16[16,2,1024,1]{2,1,0,3:T(2,128)(2,1)S(1)} %fusion.26), kind=kOutput, calls=%fused_computation.33 | convolution fusion | flops 8388608 | bytes 8470528 | tf_op jit(solution)/shard_map/shl,shld->shd/dot_general | solution.py:44
  43.6 0.1 add_convert_fusion.1
  43.7 2.1 %fusion.46 = f32[16,2048]{1,0:T(8,128)} fusion(bf16[256,2048]{1,0:T(8,128)(2,1)} %param.34, bf16[2,8,2,128]{3,2,1,0:T(2,128)(2,1)S(1)} %bitcast.56), kind=kOutput, calls=%fused_computation.66 | convolution fusion | flops 16777216 | bytes 1187840 | tf_op jit(solution)/shard_map/dot_general | solution.py:102
  45.8 0.0 reduce-scatter.4.cloned.1.call-update
  45.8 0.1 fusion.53
  45.9 0.2 select_reduce_fusion.2
  46.2 0.1 convolution_convert_fusion.2
  46.3 0.1 all_to_all.25
  46.4 0.6 copy.49
  47.0 3.7 %all-to-all-start.1 = ((bf16[4,8,4]{1,2,0:T(4,128)(2,1)}), bf16[4,8,4]{1,2,0:T(4,128)(2,1)S(1)}, u32[]{:S(2)}, u32[]{:S(2)}) async-start(bf16[4,8,4]{1,2,0:T(4,128)(2,1)} %copy.49), calls=%async_computation.2 | async-start | bytes 8192 | tf_op jit(solution)/shard_map/all_to_all | solution.py:130
  50.8 26.8 %reduce-scatter.4.cloned.1.call-done = f32[16,256]{1,0:T(8,128)} async-done(((f32[16,2048]{1,0:T(8,128)}), f32[16,256]{1,0:T(8,128)}) %reduce-scatter.4.cloned.1.call-update) | async-done | bytes 16400 | tf_op jit(solution)/shard_map/reduce_scatter | solution.py:107
  77.6 0.7 add_convert_fusion
  78.3 13.9 %all_gather.7 = bf16[16,2048]{1,0:T(8,128)(2,1)S(1)} all-gather(bf16[16,256]{1,0:T(8,128)(2,1)S(1)} %add_convert_fusion), channel_id=1, replica_groups=mesh['ep'=4,'tp'=8] {'tp'}, dimensions={1}, use_global_device_ids=true | all-gather | bytes 73728 | tf_op jit(solution)/shard_map/all_gather | solution.py:109
  92.2 0.1 fusion.15
  92.4 0.9 fusion
  93.2 3.6 %all-to-all-start = ((bf16[4,8,2048]{2,1,0:T(8,128)(2,1)}), bf16[4,8,2048]{2,1,0:T(8,128)(2,1)S(1)}, u32[]{:S(2)}, u32[]{:S(2)}) async-start(bf16[4,8,2048]{2,1,0:T(8,128)(2,1)} %fusion), calls=%async_computation.1 | async-start | bytes 262144 | tf_op jit(solution)/shard_map/all_to_all | solution.py:129
  96.9 0.1 select_reduce_fusion.1
  97.0 0.1 mul.181
  97.1 4.8 %all-to-all-done = bf16[4,8,2048]{2,1,0:T(8,128)(2,1)S(1)} async-done(((bf16[4,8,2048]{2,1,0:T(8,128)(2,1)}), bf16[4,8,2048]{2,1,0:T(8,128)(2,1)S(1)}, u32[]{:S(2)}, u32[]{:S(2)}) %all-to-all-start) | async-done | bytes 131104 | tf_op jit(solution)/shard_map/all_to_all | solution.py:129
  101.9 1.5 fusion.10
  103.4 0.0 copy-done
  103.4 2.7 %fusion.4 = f32[32,2048]{1,0:T(8,128)} fusion(bf16[1,256,2048]{2,1,0:T(8,128)(2,1)S(1)} %copy-done, bf16[1,2048,256]{2,1,0:T(8,128)(2,1)} %param.41, bf16[4,8,2048]{2,1,0:T(8,128)(2,1)S(1)} %all-to-all-done, f32[32,256]{1,0:T(8,128)S(1)} %fusion.10, f32[32]{0:T(128)S(1)} %mul.181), kind=kOutput, calls=%fused_computation.7 | convolution fusion | flops 67166208 | bytes 2523264 | tf_op jit(solution)/shard_map/dot_general | solution.py:145
  106.1 0.0 reduce-scatter.6.cloned.1.call-update
  106.1 0.0 reduce-scatter.8.cloned.1.call-start
  106.2 1.5 fusion.44
  107.6 0.0 reduce-scatter.8.cloned.1.call-update
  107.7 26.1 %reduce-scatter.6.cloned.1.call-done = f32[32,256]{1,0:T(8,128)} async-done(((f32[32,2048]{1,0:T(8,128)}), f32[32,256]{1,0:T(8,128)}) %reduce-scatter.6.cloned.1.call-update) | async-done | bytes 32784 | tf_op jit(solution)/shard_map/reduce_scatter | solution.py:147
  133.7 1.4 convert_bitcast_fusion
  135.1 3.6 %all-to-all-start.2 = ((bf16[4,8,256]{2,1,0:T(8,128)(2,1)}), bf16[4,8,256]{2,1,0:T(8,128)(2,1)S(1)}, u32[]{:S(2)}, u32[]{:S(2)}) async-start(bf16[4,8,256]{2,1,0:T(8,128)(2,1)} %convert_bitcast_fusion), calls=%async_computation.4 | async-start | bytes 32768 | tf_op jit(solution)/shard_map/all_to_all | solution.py:150
  138.7 26.0 %reduce-scatter.8.cloned.1.call-done = f32[16,256]{1,0:T(8,128)} async-done(((f32[16,2048]{1,0:T(8,128)}), f32[16,256]{1,0:T(8,128)}) %reduce-scatter.8.cloned.1.call-update) | async-done | bytes 16400 | tf_op jit(solution)/shard_map/reduce_scatter | solution.py:148
  164.7 1.5 fusion.5
  (35 shorter events, 0.2 us)
Async XLA Ops:
  7.2 96.2 %copy-start = (bf16[1,256,2048]{2,1,0:T(8,128)(2,1)S(1)}, bf16[1,256,2048]{2,1,0:T(8,128)(2,1)}, u32[]{:S(2)}) copy-start(bf16[1,256,2048]{2,1,0:T(8,128)(2,1)} %param.42) | copy-start | bytes 3145732
  7.2 31.3 %copy-start.5 = (f32[2048]{0:T(1024)S(1)}, f32[2048]{0:T(1024)}, u32[]{:S(2)}) copy-start(f32[2048]{0:T(1024)} %param.28) | copy-start | bytes 24580
  7.2 30.3 %copy-start.4 = (f32[16,2,1024]{2,1,0:T(2,128)S(1)}, f32[16,2,1024]{2,1,0:T(2,128)}, u32[]{:S(2)}) copy-start(f32[16,2,1024]{2,1,0:T(2,128)} %param.26) | copy-start | bytes 393220
  7.2 31.3 %copy-start.3 = (bf16[2048,256]{1,0:T(8,128)(2,1)S(1)}, bf16[2048,256]{1,0:T(8,128)(2,1)}, u32[]{:S(2)}) copy-start(bf16[2048,256]{1,0:T(8,128)(2,1)} %param.31) | copy-start | bytes 3145732
  7.2 70.3 %reduce-scatter.4.cloned.1.call-start = ((), (), s32[]{:S(2)}) async-start(), calls=%async_computation.6 | async-start | bytes 147456 | tf_op jit(solution)/shard_map/reduce_scatter | solution.py:107
  31.1 12.5 %copy-start.11 = (f32[16,2]{0,1:T(2,128)}, f32[16,2]{0,1:T(2,128)S(1)}, u32[]{:S(2)}) copy-start(f32[16,2]{0,1:T(2,128)S(1)} %fusion.58) | copy-start | bytes 388
  37.5 8.3 %copy-start.9 = (s32[16,1]{0,1:T(1,128)S(1)}, s32[16,1]{0,1:T(1,128)}, u32[]{:S(2)}) copy-start(s32[16,1]{0,1:T(1,128)} %param.36) | copy-start | bytes 196
  37.5 8.6 %copy-start.12 = (f32[16,2]{0,1:T(2,128)S(1)}, f32[16,2]{0,1:T(2,128)}, u32[]{:S(2)}) copy-start(f32[16,2]{0,1:T(2,128)} %param.39) | copy-start | bytes 388
  37.6 8.6 %copy-start.14 = (f32[16]{0:T(128)S(1)}, f32[16]{0:T(128)}, u32[]{:S(2)}) copy-start(f32[16]{0:T(128)} %param.38) | copy-start | bytes 196
  37.6 8.6 %copy-start.10 = (s32[16,2]{0,1:T(2,128)S(1)}, s32[16,2]{0,1:T(2,128)}, u32[]{:S(2)}) copy-start(s32[16,2]{0,1:T(2,128)} %param.37) | copy-start | bytes 388
  37.6 40.0 %copy-start.8 = (bf16[16,256]{1,0:T(8,128)(2,1)S(1)}, bf16[16,256]{1,0:T(8,128)(2,1)}, u32[]{:S(2)}) copy-start(bf16[16,256]{1,0:T(8,128)(2,1)} %param.23) | copy-start | bytes 24580
  37.6 54.8 %copy-start.6 = (f32[2048]{0:T(1024)S(1)}, f32[2048]{0:T(1024)}, u32[]{:S(2)}) copy-start(f32[2048]{0:T(1024)} %param.35) | copy-start | bytes 24580
  38.8 67.3 %copy-start.7 = (bf16[16,2,128]{2,1,0:T(2,128)(2,1)}, bf16[16,2,128]{2,1,0:T(2,128)(2,1)S(1)}, u32[]{:S(2)}) copy-start(bf16[16,2,128]{2,1,0:T(2,128)(2,1)S(1)} %convert_element_type.102) | copy-start | bytes 24580
  38.8 67.3 %copy-start.1 = (bf16[256,2048]{1,0:T(8,128)(2,1)S(1)}, bf16[256,2048]{1,0:T(8,128)(2,1)}, u32[]{:S(2)}) copy-start(bf16[256,2048]{1,0:T(8,128)(2,1)} %param.44) | copy-start | bytes 3145732
  38.8 67.3 %copy-start.2 = (bf16[2048,256]{1,0:T(8,128)(2,1)S(1)}, bf16[2048,256]{1,0:T(8,128)(2,1)}, u32[]{:S(2)}) copy-start(bf16[2048,256]{1,0:T(8,128)(2,1)} %param.43) | copy-start | bytes 3145732
  38.9 99.9 %copy-start.13 = (f32[256]{0:T(256)S(1)}, f32[256]{0:T(256)}, u32[]{:S(2)}) copy-start(f32[256]{0:T(256)} %param.45) | copy-start | bytes 3076
  47.0 46.2 %all-to-all-start.1 = ((bf16[4,8,4]{1,2,0:T(4,128)(2,1)}), bf16[4,8,4]{1,2,0:T(4,128)(2,1)S(1)}, u32[]{:S(2)}, u32[]{:S(2)}) async-start(bf16[4,8,4]{1,2,0:T(4,128)(2,1)} %copy.49), calls=%async_computation.2 | async-start | bytes 8192 | tf_op jit(solution)/shard_map/all_to_all | solution.py:130
  93.2 8.7 %all-to-all-start = ((bf16[4,8,2048]{2,1,0:T(8,128)(2,1)}), bf16[4,8,2048]{2,1,0:T(8,128)(2,1)S(1)}, u32[]{:S(2)}, u32[]{:S(2)}) async-start(bf16[4,8,2048]{2,1,0:T(8,128)(2,1)} %fusion), calls=%async_computation.1 | async-start | bytes 262144 | tf_op jit(solution)/shard_map/all_to_all | solution.py:129
  96.9 36.9 %reduce-scatter.6.cloned.1.call-start = ((), (), s32[]{:S(2)}) async-start(), calls=%async_computation.7 | async-start | bytes 294912 | tf_op jit(solution)/shard_map/reduce_scatter | solution.py:147
  106.1 58.6 %reduce-scatter.8.cloned.1.call-start = ((), (), s32[]{:S(2)}) async-start(), calls=%async_computation.8 | async-start | bytes 147456 | tf_op jit(solution)/shard_map/reduce_scatter | solution.py:148
  135.1 29.6 %all-to-all-start.2 = ((bf16[4,8,256]{2,1,0:T(8,128)(2,1)}), bf16[4,8,256]{2,1,0:T(8,128)(2,1)S(1)}, u32[]{:S(2)}, u32[]{:S(2)}) async-start(bf16[4,8,256]{2,1,0:T(8,128)(2,1)} %convert_bitcast_fusion), calls=%async_computation.4 | async-start | bytes 32768 | tf_op jit(solution)/shard_map/all_to_all | solution.py:150
Sparse Core Ops, SparseCore 0:
  45.9 31.5 reduce-scatter.3
  106.2 27.4 reduce-scatter.5
  136.0 28.7 reduce-scatter.7
where the time goes:
time: 174 us; the launch traced here: 173 us
  waiting for transfers between devices  83.8 us (48%)
  blocking collectives  29.8 us (17%)
  matrix products  24.9 us (14%)
  between operations  14 us (8%)
  starting transfers between devices  11 us (6%)
  other arithmetic  7.35 us (4%)
  local copies, waits for them, and re-layouts  1.82 us (1%)
    reduce_scatter x1, waiting for transfers between devices, body(): lax.psum_scatter(partial_value, 'tp', scatter_dimension=1, tiled=True)  26.8 us
    reduce_scatter x1, waiting for transfers between devices, body(): lax.psum_scatter(expert_part, 'tp', scatter_dimension=1, tiled=True)  26.1 us
    reduce_scatter x1, waiting for transfers between devices, body(): lax.psum_scatter(dense_part, 'tp', scatter_dimension=1, tiled=True)  26 us
    all_gather x1, blocking collectives, body(): gathered = lax.all_gather(tokens, 'tp', axis=1, tiled=True)  15.9 us
    all_gather x1, blocking collectives, body(): lax.all_gather(own_residual, 'tp', axis=1, tiled=True)  13.9 us
    dot_general x1, matrix products, attend(): jnp.einsum('shd,shld->shl', queries, key_cache, preferred_element_type=jn...  5.63 us
    all_to_all x1, waiting for transfers between devices, body(): lax.all_to_all(send_rows, 'ep', split_axis=0, concat_axis=0, tiled=True)  4.85 us
    dot_general x1, matrix products, attend(): jnp.einsum('shl,shld->shd', weights, value_cache, preferred_element_type=...  4.72 us
  transfers between devices with their start and end apart: 6, of which 4 were waited for; matrix products, arithmetic and copies ran while one was open for 3% of the time, Pallas kernels for 0%

commit v1 on v0

v1 whole, which is shorter than its diff:
```python
import functools
import jax
import jax.numpy as jnp
from jax import lax
from jax.experimental import pallas as pl
from jax.experimental.pallas import tpu as pltpu
from jax.sharding import PartitionSpec as P

FFE = 512
EPG = 4
EPS = 1e-06
FLOOR = -1e30
F32 = jnp.float32
BF16 = jnp.bfloat16
MESH = pl.DeviceIdType.MESH


def mm(a, b):
    return jnp.dot(a, b, preferred_element_type=F32)


def iota(shape, dim):
    return lax.broadcasted_iota(jnp.int32, shape, dim)


def norm_rows(values, gain):
    factor = lax.rsqrt(jnp.mean(values * values, axis=-1, keepdims=True) + EPS)
    return (values * factor * gain).astype(BF16)


def head_norm(values):
    factor = lax.rsqrt(jnp.mean(values * values, axis=-1, keepdims=True) + EPS)
    return (values * factor).astype(BF16)


def kernel(
    n_ep, n_tp, seqs, heads, head_dim, stored, cap, capacity,
    tokens, key_cache, value_cache, gate_totals, lengths, attn_gain,
    w_query, w_key, w_value, w_forget, forget_bias, w_attn_out, moe_gain,
    group_ids, inner_ids, group_prob, pair_logits,
    w_expert_gate, w_expert_up, w_expert_down, w_dense_in, w_dense_out, dense_gate,
    out, new_keys, new_values, new_gates,
    kbuf, vbuf, gbuf, wq, wk, wv, wo, wg, wu, wd, wdi, wdo,
    tok_all, part_send, part_recv, res_send, res_all, sel_send, row_recv,
    rw_send, rw_recv, dense_send, dense_recv, ret_send, ret_recv,
    k_sem, v_sem, w_sem,
    tok_s, tok_r, rw_s, rw_r, part_s, part_r, res_s, res_r, row_s, row_r,
    dn_s, dn_r, own_s, own_r, ret_s, ret_r,
):
    me_ep = lax.axis_index("ep")
    me_tp = lax.axis_index("tp")
    feat = tokens.shape[1]
    rows = seqs * heads
    per_group = 16 // heads
    n_groups = rows // 16

    def tp_peer(d):
        return lax.rem(me_tp + d, n_tp)

    def ep_peer(d):
        return lax.rem(me_ep + d, n_ep)

    def remote(src, dst, send, recv, ep, tp):
        return pltpu.make_async_remote_copy(
            src_ref=src, dst_ref=dst, send_sem=send, recv_sem=recv,
            device_id=(ep, tp), device_id_type=MESH,
        )

    local = []

    def load(src, dst, sem):
        copy = pltpu.make_async_copy(src, dst, sem)
        copy.start()
        return copy

    c_wq = load(w_query, wq, w_sem.at[0])
    c_wk = load(w_key, wk, w_sem.at[1])
    c_wv = load(w_value, wv, w_sem.at[2])
    c_gt = load(gate_totals, gbuf, w_sem.at[3])
    c_k = [load(key_cache.at[s], kbuf.at[s], k_sem.at[s]) for s in range(seqs)]
    c_v = [load(value_cache.at[s], vbuf.at[s], v_sem.at[s]) for s in range(seqs)]
    c_wo = load(w_attn_out, wo, w_sem.at[4])
    c_wdi = load(w_dense_in, wdi, w_sem.at[5])
    c_wdo = load(w_dense_out, wdo, w_sem.at[6])
    c_wg = load(w_expert_gate.at[0], wg, w_sem.at[7])
    c_wu = load(w_expert_up.at[0], wu, w_sem.at[8])
    c_wd = load(w_expert_down.at[0], wd, w_sem.at[9])

    barrier = pltpu.get_barrier_semaphore()
    total = n_ep * n_tp
    me = me_ep * n_tp + me_tp

    def greet(i, carry):
        other = lax.rem(me + i, total)
        pl.semaphore_signal(
            barrier, inc=1, device_id=(other // n_tp, lax.rem(other, n_tp)), device_id_type=MESH
        )
        return carry

    lax.fori_loop(1, total, greet, 0)

    eye = iota((seqs, seqs), 0) == iota((seqs, seqs), 1)
    gid_col = group_ids[...]
    gid_sq = jnp.broadcast_to(gid_col, (seqs, seqs))
    gid_row = jnp.sum(jnp.where(eye, gid_sq, 0).astype(F32), axis=0, keepdims=True).astype(jnp.int32)
    same = gid_sq == gid_row
    later = iota((seqs, seqs), 0) > iota((seqs, seqs), 1)
    sooner = iota((seqs, seqs), 0) < iota((seqs, seqs), 1)
    slot_col = jnp.sum(jnp.where(same & later, 1.0, 0.0), axis=1, keepdims=True).astype(jnp.int32)
    slot_row = jnp.sum(jnp.where(same & sooner, 1.0, 0.0), axis=0, keepdims=True).astype(jnp.int32)
    pos_col = gid_col * cap + slot_col
    pos_row = gid_row * cap + slot_row
    pick = jnp.where(iota((n_ep * cap, seqs), 0) == pos_row, 1.0, 0.0).astype(BF16)
    pick_own = jnp.where(iota((cap, seqs), 0) + me_ep * cap == pos_row, 1.0, 0.0).astype(BF16)
    put = jnp.where(iota((seqs, n_ep * cap), 1) == pos_col, 1.0, 0.0).astype(BF16)

    def column_of(row):
        return jnp.sum(jnp.where(eye, jnp.broadcast_to(row, (seqs, seqs)), 0.0), axis=1, keepdims=True)

    logits = pair_logits[...]
    first = jax.nn.sigmoid(logits[:, 0:1] - logits[:, 1:2])
    prob = column_of(group_prob[...])
    lane = iota((seqs, 128), 1)
    picked = inner_ids[...]
    spread = jnp.where(picked[:, 0:1] == lane, prob * first, 0.0) + jnp.where(
        picked[:, 1:2] == lane, prob * (1.0 - first), 0.0
    )
    routed = mm(pick, spread.astype(BF16))
    for e in range(n_ep):
        rw_send[e] = routed[e * cap:(e + 1) * cap].astype(BF16)
    rw_recv[me_ep] = mm(pick_own, spread.astype(BF16)).astype(BF16)
    tok_all[me_tp] = tokens[...]

    pl.semaphore_wait(barrier, total - 1)

    for d in range(1, n_tp):
        p = tp_peer(d)
        remote(tokens, tok_all.at[me_tp], tok_s.at[d], tok_r.at[me_tp], me_ep, p).start()
    for d in range(1, n_ep):
        e = ep_peer(d)
        remote(rw_send.at[e], rw_recv.at[me_ep], rw_s.at[d], rw_r.at[me_ep], e, me_tp).start()
    for d in range(1, n_tp):
        p = tp_peer(d)
        remote(tokens, tok_all.at[p], tok_s.at[d], tok_r.at[p], me_ep, p).wait_recv()

    x = jnp.concatenate([tok_all[t].astype(F32) for t in range(n_tp)], axis=1)
    normed = norm_rows(x, attn_gain[...])
    c_wq.wait()
    zq = mm(normed, wq[...])
    c_wk.wait()
    zk = mm(normed, wk[...])
    c_wv.wait()
    zv = mm(normed, wv[...])
    gate_pre = mm(normed, w_forget[...]) + forget_bias[...]
    log_gate = jnp.minimum(gate_pre, 0.0) - jnp.log1p(jnp.exp(-jnp.abs(gate_pre)))

    q_rows = k_rows = v_rows = jnp.zeros((rows, head_dim), F32)
    for h in range(heads):
        place = jnp.where(
            iota((rows, seqs), 0) == iota((rows, seqs), 1) * heads + h, 1.0, 0.0
        ).astype(BF16)
        cols = slice(h * head_dim, (h + 1) * head_dim)
        q_rows = q_rows + mm(place, head_norm(zq[:, cols]))
        k_rows = k_rows + mm(place, head_norm(zk[:, cols]))
        v_rows = v_rows + mm(place, zv[:, cols].astype(BF16))
    new_keys[...] = k_rows.astype(BF16)
    new_values[...] = v_rows.astype(BF16)

    n_heads = log_gate.shape[1]
    row_seq = iota((rows, n_heads), 0) // heads
    lg_rows = jnp.zeros((rows, n_heads), F32)
    for s in range(seqs):
        lg_rows = jnp.where(row_seq == s, log_gate[s:s + 1, :], lg_rows)
    row_head = me_tp * heads + lax.rem(iota((rows, n_heads), 0), heads)
    lg_rows = jnp.sum(
        jnp.where(iota((rows, n_heads), 1) == row_head, lg_rows, 0.0), axis=1, keepdims=True
    )
    len_rows = jnp.sum(
        jnp.where(
            iota((rows, seqs), 1) == iota((rows, seqs), 0) // heads,
            jnp.broadcast_to(lengths[...].astype(F32), (rows, seqs)), 0.0,
        ),
        axis=1, keepdims=True,
    ).astype(jnp.int32)

    c_gt.wait()
    scale = head_dim ** (-0.5)
    wide_row = iota((16, stored), 0)
    entry = iota((16, stored), 1)
    slim_row = iota((16, head_dim), 0)
    att_list, ng_list = [], []
    for g in range(n_groups):
        here = slice(g * 16, (g + 1) * 16)
        q = q_rows[here]
        q_low = q.astype(BF16)
        scores = jnp.zeros((16, stored), F32)
        totals = jnp.zeros((16, stored), F32)
        for j in range(per_group):
            s = g * per_group + j
            c_k[s].wait()
            block = kbuf[s].reshape(heads * stored, head_dim)
            product = lax.dot_general(
                q_low, block, (((1,), (1,)), ((), ())), preferred_element_type=F32
            )
            for h in range(heads):
                at = wide_row == j * heads + h
                scores = jnp.where(at, product[:, h * stored:(h + 1) * stored], scores)
                totals = jnp.where(at, gbuf[s, h:h + 1, :], totals)
        length = len_rows[here]
        last = jnp.sum(jnp.where(entry == length - 1, totals, 0.0), axis=1, keepdims=True)
        current = last + lg_rows[here]
        ng_list.append(current)
        live = entry < length
        scores = jnp.where(live, scores * scale + current - totals, FLOOR)
        own_score = jnp.sum(q * k_rows[here], axis=1, keepdims=True) * scale
        peak = jnp.maximum(jnp.max(scores, axis=1, keepdims=True), own_score)
        terms = jnp.where(live, jnp.exp(scores - peak), 0.0)
        own_term = jnp.exp(own_score - peak)
        denom = jnp.sum(terms, axis=1, keepdims=True) + own_term
        weights = (terms / denom).astype(BF16)
        own_weight = (own_term / denom).astype(BF16).astype(F32)
        att = jnp.zeros((16, head_dim), F32)
        for j in range(per_group):
            s = g * per_group + j
            c_v[s].wait()
            for h in range(heads):
                att = jnp.where(slim_row == j * heads + h, mm(weights, vbuf[s, h]), att)
        att_list.append(att + own_weight * v_rows[here])
    att_rows = jnp.concatenate(att_list, axis=0).astype(BF16) if n_groups > 1 else att_list[0].astype(BF16)
    ng_col = jnp.concatenate(ng_list, axis=0) if n_groups > 1 else ng_list[0]

    pieces = []
    for h in range(heads):
        place = jnp.where(
            iota((seqs, rows), 1) == iota((seqs, rows), 0) * heads + h, 1.0, 0.0
        ).astype(BF16)
        pieces.append(mm(place, att_rows))
    attended = (jnp.concatenate(pieces, axis=1) if heads > 1 else pieces[0]).astype(BF16)

    c_wo.wait()
    projected = mm(attended, wo[...])
    for t in range(n_tp):
        part_send[t] = projected[:, t * feat:(t + 1) * feat].astype(BF16)
    for d in range(1, n_tp):
        p = tp_peer(d)
        remote(part_send.at[p], part_recv.at[me_tp], part_s.at[d], part_r.at[me_tp], me_ep, p).start()
    part_recv[me_tp] = part_send[me_tp]

    ng_row = jnp.sum(
        jnp.where(iota((rows, rows), 0) == iota((rows, rows), 1), jnp.broadcast_to(ng_col, (rows, rows)), 0.0),
        axis=0, keepdims=True,
    )
    ng = jnp.zeros((seqs, heads), F32)
    for h in range(heads):
        col = jnp.sum(
            jnp.where(iota((seqs, rows), 1) == iota((seqs, rows), 0) * heads + h, ng_row, 0.0),
            axis=1, keepdims=True,
        )
        ng = jnp.where(iota((seqs, heads), 1) == h, col, ng)
    new_gates[...] = ng

    for d in range(1, n_tp):
        p = tp_peer(d)
        remote(part_send.at[p], part_recv.at[p], part_s.at[d], part_r.at[p], me_ep, p).wait_recv()
    summed = part_recv[0].astype(F32)
    for t in range(1, n_tp):
        summed = summed + part_recv[t].astype(F32)
    residual = (tokens[...].astype(F32) + summed).astype(BF16)

    res_send[...] = residual
    for d in range(1, n_tp):
        p = tp_peer(d)
        remote(res_send, res_all.at[me_tp], res_s.at[d], res_r.at[me_tp], me_ep, p).start()
    chosen = mm(pick, residual)
    for e in range(n_ep):
        sel_send[e] = chosen[e * cap:(e + 1) * cap].astype(BF16)
    for d in range(1, n_ep):
        e = ep_peer(d)

        def send_rows(i, carry, e=e, d=d):
            remote(
                sel_send.at[e], row_recv.at[me_ep, me_tp], row_s.at[d], row_r.at[me_ep], e, tp_peer(i)
            ).start()
            return carry

        lax.fori_loop(0, n_tp, send_rows, 0)
    res_all[me_tp] = residual

    for d in range(1, n_tp):
        p = tp_peer(d)
        remote(res_send, res_all.at[p], res_s.at[d], res_r.at[p], me_ep, p).wait_recv()
    res_full = jnp.concatenate([res_all[t].astype(F32) for t in range(n_tp)], axis=1)
    moe_in = norm_rows(res_full, moe_gain[...])
    own_rows = mm(pick_own, res_full.astype(BF16))
    for t in range(n_tp):
        row_recv[me_ep, t] = own_rows[:, t * feat:(t + 1) * feat].astype(BF16)

    c_wdi.wait()
    dense_hidden = jax.nn.silu(mm(moe_in, wdi[...])).astype(BF16)
    c_wdo.wait()
    dense_part = mm(dense_hidden, wdo[...])
    for t in range(n_tp):
        dense_send[t] = dense_part[:, t * feat:(t + 1) * feat].astype(BF16)
    for d in range(1, n_tp):
        p = tp_peer(d)
        remote(dense_send.at[p], dense_recv.at[me_tp], dn_s.at[d], dn_r.at[me_tp], me_ep, p).start()
    dense_recv[me_tp] = dense_send[me_tp]

    for d in range(1, n_ep):
        e = ep_peer(d)
        remote(rw_send.at[e], rw_recv.at[e], rw_s.at[d], rw_r.at[e], e, me_tp).wait_recv()
        remote(row_recv.at[e], row_recv.at[e], row_s.at[d], row_r.at[e], e, me_tp).wait_recv()
    gathered = jnp.concatenate(
        [
            jnp.concatenate([row_recv[e, t].astype(F32) for t in range(n_tp)], axis=1)
            for e in range(n_ep)
        ],
        axis=0,
    )
    expert_in = norm_rows(gathered, moe_gain[...])
    route = jnp.concatenate([rw_recv[e].astype(F32) for e in range(n_ep)], axis=0)
    expert_index = me_tp * w_expert_gate.shape[2] // FFE
    route_col = jnp.sum(
        jnp.where(iota(route.shape, 1) == expert_index, route, 0.0), axis=1, keepdims=True
    )
    c_wg.wait()
    gate_mid = mm(expert_in, wg[...])
    c_wu.wait()
    up_mid = mm(expert_in, wu[...])
    hidden = (jax.nn.silu(gate_mid) * up_mid * route_col).astype(BF16)
    c_wd.wait()
    expert_part = mm(hidden, wd[...])
    for e in range(n_ep):
        for t in range(n_tp):
            ret_send[e, t] = expert_part[e * cap:(e + 1) * cap, t * feat:(t + 1) * feat].astype(BF16)
    for d in range(1, n_ep):
        e = ep_peer(d)

        def send_back(i, carry, e=e, d=d):
            p = tp_peer(i)
            remote(
                ret_send.at[e, p], ret_recv.at[me_ep, me_tp], ret_s.at[d], ret_r.at[me_ep], e, p
            ).start()
            return carry

        lax.fori_loop(0, n_tp, send_back, 0)
    for d in range(1, n_tp):
        p = tp_peer(d)
        remote(
            ret_send.at[me_ep, p], ret_recv.at[me_ep, me_tp], own_s.at[d], own_r.at[me_tp], me_ep, p
        ).start()
    ret_recv[me_ep, me_tp] = ret_send[me_ep, me_tp]

    for d in range(1, n_tp):
        p = tp_peer(d)
        remote(dense_send.at[p], dense_recv.at[p], dn_s.at[d], dn_r.at[p], me_ep, p).wait_recv()
    dense_sum = dense_recv[0].astype(F32)
    for t in range(1, n_tp):
        dense_sum = dense_sum + dense_recv[t].astype(F32)
    base = residual.astype(F32) + jax.nn.sigmoid(dense_gate[...]) * dense_sum
    for d in range(1, n_tp):
        p = tp_peer(d)
        remote(
            ret_send.at[me_ep, p], ret_recv.at[me_ep, p], own_s.at[d], own_r.at[p], me_ep, p
        ).wait_recv()
    for d in range(1, n_ep):
        e = ep_peer(d)
        remote(ret_recv.at[e], ret_recv.at[e], ret_s.at[d], ret_r.at[e], e, me_tp).wait_recv()
    sums = []
    for e in range(n_ep):
        acc = ret_recv[e, 0].astype(F32)
        for t in range(1, n_tp):
            acc = acc + ret_recv[e, t].astype(F32)
        sums.append(acc)
    expert_out = mm(put, jnp.concatenate(sums, axis=0).astype(BF16))
    out[...] = (base + expert_out).astype(BF16)

    for d in range(1, n_tp):
        p = tp_peer(d)
        remote(tokens, tok_all.at[me_tp], tok_s.at[d], tok_r.at[me_tp], me_ep, p).wait_send()
        remote(part_send.at[p], part_recv.at[me_tp], part_s.at[d], part_r.at[me_tp], me_ep, p).wait_send()
        remote(res_send, res_all.at[me_tp], res_s.at[d], res_r.at[me_tp], me_ep, p).wait_send()
        remote(dense_send.at[p], dense_recv.at[me_tp], dn_s.at[d], dn_r.at[me_tp], me_ep, p).wait_send()
        remote(
            ret_send.at[me_ep, p], ret_recv.at[me_ep, me_tp], own_s.at[d], own_r.at[me_tp], me_ep, p
        ).wait_send()
    for d in range(1, n_ep):
        e = ep_peer(d)
        remote(rw_send.at[e], rw_recv.at[me_ep], rw_s.at[d], rw_r.at[me_ep], e, me_tp).wait_send()
        remote(row_recv.at[e], row_recv.at[e], row_s.at[d], row_r.at[e], e, me_tp).wait_send()
        remote(ret_recv.at[e], ret_recv.at[e], ret_s.at[d], ret_r.at[e], e, me_tp).wait_send()


def body(n_ep, n_tp, *args):
    (
        tokens, key_cache, value_cache, gate_totals, lengths, attn_gain,
        w_query, w_key, w_value, w_forget, forget_bias, w_attn_out, moe_gain,
        group_ids, inner_ids, group_prob, pair_logits,
        w_expert_gate, w_expert_up, w_expert_down, w_dense_in, w_dense_out, dense_gate,
    ) = args
    seqs, heads, stored, head_dim = key_cache.shape
    feat = tokens.shape[1]
    capacity = max(2, 2 * seqs // n_ep)
    cap = -(-capacity // 8) * 8
    rows = seqs * heads
    vm = pl.BlockSpec(memory_space=pltpu.VMEM)
    hb = pl.BlockSpec(memory_space=pl.ANY)

    def like(a):
        return pltpu.VMEM(a.shape, a.dtype)

    def dma(*n):
        return pltpu.SemaphoreType.DMA(n)

    operands = (
        tokens, key_cache, value_cache, gate_totals, lengths.reshape(1, -1), attn_gain.reshape(1, -1),
        w_query, w_key, w_value, w_forget, forget_bias.reshape(1, -1), w_attn_out,
        moe_gain.reshape(1, -1), group_ids, inner_ids, group_prob.reshape(1, -1), pair_logits,
        w_expert_gate, w_expert_up, w_expert_down, w_dense_in, w_dense_out, dense_gate.reshape(1, -1),
    )
    specs = [vm, hb, hb, hb, vm, vm, hb, hb, hb, vm, vm, hb, vm, vm, vm, vm, vm, hb, hb, hb, hb, hb, vm]
    scratch = [
        like(key_cache), like(value_cache), like(gate_totals),
        like(w_query), like(w_key), like(w_value), like(w_attn_out),
        pltpu.VMEM(w_expert_gate.shape[1:], BF16),
        pltpu.VMEM(w_expert_up.shape[1:], BF16),
        pltpu.VMEM(w_expert_down.shape[1:], BF16),
        like(w_dense_in), like(w_dense_out),
        pltpu.VMEM((n_tp, seqs, feat), BF16),
        pltpu.VMEM((n_tp, seqs, feat), BF16),
        pltpu.VMEM((n_tp, seqs, feat), BF16),
        pltpu.VMEM((seqs, feat), BF16),
        pltpu.VMEM((n_tp, seqs, feat), BF16),
        pltpu.VMEM((n_ep, cap, feat), BF16),
        pltpu.VMEM((n_ep, n_tp, cap, feat), BF16),
        pltpu.VMEM((n_ep, cap, 128), BF16),
        pltpu.VMEM((n_ep, cap, 128), BF16),
        pltpu.VMEM((n_tp, seqs, feat), BF16),
        pltpu.VMEM((n_tp, seqs, feat), BF16),
        pltpu.VMEM((n_ep, n_tp, cap, feat), BF16),
        pltpu.VMEM((n_ep, n_tp, cap, feat), BF16),
        dma(seqs), dma(seqs), dma(10),
        dma(n_tp), dma(n_tp), dma(n_ep), dma(n_ep), dma(n_tp), dma(n_tp),
        dma(n_tp), dma(n_tp), dma(n_ep), dma(n_ep),
        dma(n_tp), dma(n_tp), dma(n_tp), dma(n_tp), dma(n_ep), dma(n_ep),
    ]
    out, keys, values, gates = pl.pallas_call(
        functools.partial(kernel, n_ep, n_tp, seqs, heads, head_dim, stored, cap, capacity),
        out_shape=(
            jax.ShapeDtypeStruct((seqs, feat), BF16),
            jax.ShapeDtypeStruct((rows, head_dim), BF16),
            jax.ShapeDtypeStruct((rows, head_dim), BF16),
            jax.ShapeDtypeStruct((seqs, heads), F32),
        ),
        in_specs=specs,
        out_specs=(vm, vm, vm, vm),
        scratch_shapes=scratch,
        compiler_params=pltpu.CompilerParams(
            collective_id=0, has_side_effects=True, vmem_limit_bytes=56 * 1024 * 1024
        ),
    )(*operands)
    shape = (seqs, heads, head_dim)
    return out, keys.reshape(shape), values.reshape(shape), gates


def solution(mesh):
    placed = (
        P("ep", "tp"),
        P("ep", "tp", None, None),
        P("ep", "tp", None, None),
        P("ep", "tp", None),
        P("ep"),
        P(),
        P(None, "tp"),
        P(None, "tp"),
        P(None, "tp"),
        P(),
        P(),
        P("tp", None),
        P(),
        P("ep", None),
        P("ep", None),
        P("ep"),
        P("ep", None),
        P("ep", None, "tp"),
        P("ep", None, "tp"),
        P("ep", "tp", None),
        P(None, "tp"),
        P("tp", None),
        P("tp"),
    )
    return jax.shard_map(
        functools.partial(body, mesh.shape["ep"], mesh.shape["tp"]),
        mesh=mesh,
        in_specs=placed,
        out_specs=(P("ep", "tp"), P("ep", "tp", None), P("ep", "tp", None), P("ep", "tp")),
        check_vma=False,
    )
```

time: 174 us -> 51.8 us (0.30)
  waiting for transfers between devices: 83.8 us -> 0 us
  Pallas kernels: 0 us -> 39.6 us
  blocking collectives: 29.8 us -> 0 us
  matrix products: 24.9 us -> 0 us
  between operations: 14 us -> 0.64 us
  starting transfers between devices: 11 us -> 0 us
  local copies, waits for them, and re-layouts: 1.82 us -> 11.1 us
  other arithmetic: 7.35 us -> 0 us
    reduce_scatter x3 -> x0, waiting for transfers between devices: 78.9 us -> none  [the longest x1 26.8 us: body(): lax.psum_scatter(partial_value, 'tp', scatter_dimension=1, tiled=True)]
    pallas_call x0 -> x1, Pallas kernels: none -> 39.6 us  [body(): pl.pallas_call(functools.partial(kernel, n_ep, n_tp, seqs, heads, head_di...]
    all_gather x2 -> x0, blocking collectives: 29.8 us -> none  [the longest x1 15.9 us: body(): gathered = lax.all_gather(tokens, 'tp', axis=1, tiled=True)]
    dot_general x13 -> x0, matrix products: 24.9 us -> none  [the longest x1 5.63 us: attend(): jnp.einsum('shd,shld->shl', queries, key_cache, preferred_element_type=jn...]
    unnamed x30 -> x8, local copies, waits for them, and re-layouts: 0.1 us -> 11.1 us
    all_to_all x3 -> x0, starting transfers between devices: 11 us -> none  [the longest x1 3.72 us: body(): lax.all_to_all(send_weights, 'ep', split_axis=0, concat_axis=0, tiled=True)]
    all_to_all x3 -> x0, waiting for transfers between devices: 4.85 us -> none  [the longest x1 4.85 us: body(): lax.all_to_all(send_rows, 'ep', split_axis=0, concat_axis=0, tiled=True)]
    reduce_sum x10 -> x0, other arithmetic: 2.8 us -> none  [the longest x1 1.08 us: body(): new_gates = jnp.sum(jnp.where(at_last, gate_totals, 0.0), axis=2) + log_gate]
  transfers between devices with their start and end apart: 6 -> 0, of which waited for: 4 -> 0; matrix products, arithmetic and copies ran while one was open for 3% -> 0% of each run, Pallas kernels for 0% -> 0%
where the time goes in v1:
time: 51.8 us; the launch traced here: 51.3 us
  Pallas kernels  39.6 us (76%)
  local copies, waits for them, and re-layouts  11.1 us (21%)
  between operations  0.64 us (1%)
    pallas_call x1, Pallas kernels, body(): pl.pallas_call(functools.partial(kernel, n_ep, n_tp, seqs, heads, head_di...  39.6 us
    unnamed x8, local copies, waits for them, and re-layouts  11.1 us

profile of v1, /device:TPU:0, one launch (start us, length us, event | category | flops | bytes accessed | tf_op | source)
XLA Modules:
  0.0 51.3 jit_solution(1849099025311786374)
XLA Ops:
  0.6 1.3 %copy.28.group_ids = s32[16,1]{1,0:T(8,128)} copy(s32[16,1]{0,1:T(1,128)} %param.36) | data formatting | bytes 128 | tf_op args[13]
  2.0 1.4 %copy.29.inner_ids = s32[16,2]{1,0:T(8,128)} copy(s32[16,2]{0,1:T(2,128)} %param.37) | data formatting | bytes 256 | tf_op args[14]
  3.3 1.4 %copy.30.pair_logits = f32[16,2]{1,0:T(8,128)} copy(f32[16,2]{0,1:T(2,128)} %param.39) | data formatting | bytes 256 | tf_op args[16]
  4.7 1.8 %copy.27.w_forget = bf16[2048,16]{1,0:T(8,128)(2,1)} copy(bf16[2048,16]{0,1:T(8,128)(2,1)} %param.32) | data formatting | bytes 131072 | tf_op args[9]
  6.5 39.6 %shard_map.246 = (bf16[16,256]{1,0:T(8,128)(2,1)}, bf16[32,128]{1,0:T(8,128)(2,1)}, bf16[32,128]{1,0:T(8,128)(2,1)}, f32[16,2]{1,0:T(8,128)}) custom-call(bf16[16,256]{1,0:T(8,128)(2,1)} %tokens.1, bf16[16,2,1024,128]{3,2,1,0:T(8,128)(2,1)} %key_cache.1, bf16[16,2,1024,128]{3,2,1,0:T(8,128)(2,1)} %value_cache.1, f32[16,2,1024]{2,1,0:T(2,128)} %gate_totals.1, ...), custom_call_target="tpu_custom_call" | custom-call | tf_op jit(solution)/shard_map/pallas_call | solution.py:447
  46.1 1.3 %copy.31 = f32[16,2]{0,1:T(2,128)} copy(f32[16,2]{1,0:T(8,128)} %get-tuple-element.15) | data formatting | bytes 256
  47.4 1.3 %copy.35 = bf16[16,256]{1,0:T(8,128)(2,1)} copy(bf16[16,256]{1,0:T(8,128)(2,1)} %get-tuple-element.20) | data formatting | bytes 16384
  48.7 1.3 %copy.36 = bf16[16,2,128]{2,1,0:T(2,128)(2,1)} copy(bf16[16,2,128]{2,1,0:T(2,128)(2,1)} %bitcast.11) | data formatting | bytes 16384
  50.0 1.3 %copy.37 = bf16[16,2,128]{2,1,0:T(2,128)(2,1)} copy(bf16[16,2,128]{2,1,0:T(2,128)(2,1)} %bitcast.10) | data formatting | bytes 16384
